TPU v7x, 32 devices: a whole 2x2x4 slice. The times are simulated.
32 devices in a mesh: fs: 4 (over y, x), tp: 8 (over z, core).
Axes of the slice: x: 2, y: 2, z: 4, core: 2. Of those that a mesh axis runs over, the one named last changes fastest.
Arguments:
- stream_in: bfloat16 [4096, 4096], P(('fs', 'tp')), may hold values from -6 to 6
- mixer_out: bfloat16 [4096, 4096], P(('fs', 'tp')), may hold values from -6 to 6
- mix_gain: float32 [4096], replicated, may hold values from 0.1 to 1.9
- pre_gain: float32 [4096], replicated, may hold values from 0.1 to 1.9
- gate_weight: float32 [4096, 6144], P('fs', 'tp'), may hold values from -0.09375 to 0.09375
- up_weight: float32 [4096, 6144], P('fs', 'tp'), may hold values from -0.09375 to 0.09375
- gate_scale: float32 [6144], P('tp'), may hold values from 0.5 to 2
- up_scale: float32 [6144], P('tp'), may hold values from 0.5 to 2
Outputs:
- hidden: bfloat16 [4096, 6144], P('fs', 'tp')
- stream: bfloat16 [4096, 4096], P(('fs', 'tp'))
All inputs are finite; a program needn't handle non-finite values.
Results may differ from a plain program's by a relative error of at most 0.0082.
Values may be sent and summed in bfloat16 or wider, within the bound.
A program may use at most 128 MiB of HBM per device.

v0:
```python
import jax
import jax.numpy as jnp
from jax import lax
from jax.sharding import PartitionSpec as P

epsilon = 1e-06


def rms_scaled(values, gain):
    return values * lax.rsqrt(jnp.mean(values * values, axis=-1, keepdims=True) + epsilon) * gain


def on_device(
    stream_in, mixer_out, mix_gain, pre_gain, gate_weight, up_weight, gate_scale, up_scale
):
    mixed = stream_in.astype(jnp.float32) + rms_scaled(mixer_out.astype(jnp.float32), mix_gain)
    stream = mixed.astype(jnp.bfloat16)
    normed = rms_scaled(stream.astype(jnp.float32), pre_gain).astype(jnp.bfloat16)
    gate_cast = gate_weight.astype(jnp.bfloat16)
    up_cast = up_weight.astype(jnp.bfloat16)
    gate_full, up_full = (
        lax.all_gather(gate_cast, "fs", axis=0, tiled=True),
        lax.all_gather(up_cast, "fs", axis=0, tiled=True),
    )
    piece = lax.all_gather(normed, "tp", axis=0, tiled=True)
    gate = jnp.dot(piece, gate_full, preferred_element_type=jnp.float32) * gate_scale
    up = jnp.dot(piece, up_full, preferred_element_type=jnp.float32) * up_scale
    hidden = (jax.nn.silu(gate) * up).astype(jnp.bfloat16)
    return (hidden, stream)


def solution(mesh):
    return jax.shard_map(
        on_device,
        mesh=mesh,
        in_specs=(
            P(("fs", "tp"), None),
            P(("fs", "tp"), None),
            P(),
            P(),
            P("fs", "tp"),
            P("fs", "tp"),
            P("tp"),
            P("tp"),
        ),
        out_specs=(P("fs", "tp"), P(("fs", "tp"), None)),
        check_vma=False,
    )
```

profile of v0, /device:TPU:0, one launch (start us, length us, event | category | flops | bytes accessed | tf_op | source)
XLA Modules:
  0.0 256.1 jit_solution(6884719773406794379)
XLA Ops:
  7.2 0.0 copy-start.1
  7.2 0.0 copy-start.3
  7.2 0.0 all-gather.6.cloned.1.call-start
  7.2 3.3 %convert_element_type.29 = bf16[1024,768]{1,0:T(8,128)(2,1)} convert(f32[1024,768]{1,0:T(8,128)} %param.12) | non-fusion elementwise | flops 786432 | bytes 4718592 | tf_op jit(solution)/shard_map/convert_element_type | solution.py:19
  10.6 0.0 all-gather.6.cloned.1.call-update
  10.6 0.0 all-gather.4.cloned.1.call-start
  10.6 0.0 copy-done.1
  10.6 0.3 fusion
  11.0 0.7 fusion.4
  11.7 0.0 copy-start
  11.7 0.0 copy-done.4
  11.7 1.3 fusion.6
  13.1 0.0 all-gather.4.cloned.1.call-update
  13.1 0.0 all-gather.8.cloned.1.call-start
  13.2 3.2 %convert_element_type.30 = bf16[1024,768]{1,0:T(8,128)(2,1)} convert(f32[1024,768]{1,0:T(8,128)} %param.13) | non-fusion elementwise | flops 786432 | bytes 4718592 | tf_op jit(solution)/shard_map/convert_element_type | solution.py:20
  16.4 0.0 all-gather.8.cloned.1.call-update
  16.4 0.0 copy-start.5
  16.4 0.0 copy-start.6
  16.4 67.1 %all-gather.6.cloned.1.call-done = bf16[4096,768]{1,0:T(8,128)(2,1)} async-done(((bf16[1024,768]{1,0:T(8,128)(2,1)}), bf16[4096,768]{1,0:T(8,128)(2,1)}) %all-gather.6.cloned.1.call-update) | async-done | bytes 6291472 | tf_op jit(solution)/shard_map/all_gather | solution.py:22
  83.5 83.7 %all-gather.4.cloned.1.call-done = bf16[1024,4096]{1,0:T(8,128)(2,1)} async-done(((bf16[128,4096]{1,0:T(8,128)(2,1)}), bf16[1024,4096]{1,0:T(8,128)(2,1)}) %all-gather.4.cloned.1.call-update) | async-done | bytes 8388624 | tf_op jit(solution)/shard_map/all_gather | solution.py:25
  167.2 10.9 %fusion.8 = f32[1024,768]{1,0:T(8,128)S(1)} fusion(bf16[1024,4096]{1,0:T(8,128)(2,1)} %all-gather.4.cloned.1.call-done, bf16[4096,768]{1,0:T(8,128)(2,1)} %all-gather.6.cloned.1.call-done), kind=kOutput, calls=%fused_computation.14 | convolution fusion | flops 6442450944 | bytes 17825792 | tf_op jit(solution)/shard_map/dot_general | solution.py:26
  178.1 59.5 %all-gather.8.cloned.1.call-done = bf16[4096,768]{1,0:T(8,128)(2,1)} async-done(((bf16[1024,768]{1,0:T(8,128)(2,1)}), bf16[4096,768]{1,0:T(8,128)(2,1)}) %all-gather.8.cloned.1.call-update) | async-done | bytes 6291472 | tf_op jit(solution)/shard_map/all_gather | solution.py:23
  237.6 0.0 copy-done.5
  237.6 12.1 %multiply_convert_fusion = bf16[1024,768]{1,0:T(8,128)(2,1)} fusion(f32[1024,768]{1,0:T(8,128)S(1)} %fusion.8, bf16[1024,4096]{1,0:T(8,128)(2,1)} %all-gather.4.cloned.1.call-done, bf16[4096,768]{1,0:T(8,128)(2,1)} %all-gather.8.cloned.1.call-done, f32[768]{0:T(1024)S(1)} %copy-done.5, f32[768]{0:T(1024)S(1)} %copy-done.6), kind=kOutput, calls=%fused_computation | convolution fusion | flops 6448742400 | bytes 19404800 | tf_op jit(solution)/shard_map/dot_general | solution.py:27
  (8 shorter events, 0.0 us)
Async XLA Ops:
  7.2 3.5 %copy-start.1 = (bf16[128,4096]{1,0:T(8,128)(2,1)S(1)}, bf16[128,4096]{1,0:T(8,128)(2,1)}, u32[]{:S(2)}) copy-start(bf16[128,4096]{1,0:T(8,128)(2,1)} %param.9) | copy-start | bytes 3145732
  7.2 3.8 %copy-start.3 = (f32[4096]{0:T(1024)S(1)}, f32[4096]{0:T(1024)}, u32[]{:S(2)}) copy-start(f32[4096]{0:T(1024)} %param.10) | copy-start | bytes 49156
  7.2 3.8 %copy-start.2 = (bf16[128,4096]{1,0:T(8,128)(2,1)S(1)}, bf16[128,4096]{1,0:T(8,128)(2,1)}, u32[]{:S(2)}) copy-start(bf16[128,4096]{1,0:T(8,128)(2,1)} %param.8) | copy-start | bytes 3145732
  7.2 76.3 %all-gather.6.cloned.1.call-start = ((), (), s32[]{:S(2)}) async-start(), calls=%async_computation.1 | async-start | bytes 7864320 | tf_op jit(solution)/shard_map/all_gather | solution.py:22
  10.6 1.2 copy-start.4
  10.6 156.6 %all-gather.4.cloned.1.call-start = ((), (), s32[]{:S(2)}) async-start(), calls=%async_computation | async-start | bytes 9437184 | tf_op jit(solution)/shard_map/all_gather | solution.py:25
  11.7 4.7 %copy-start = (bf16[128,4096]{1,0:T(8,128)(2,1)}, bf16[128,4096]{1,0:T(8,128)(2,1)S(1)}, u32[]{:S(2)}) copy-start(bf16[128,4096]{1,0:T(8,128)(2,1)S(1)} %get-tuple-element.3) | copy-start | bytes 3145732
  13.1 224.4 %all-gather.8.cloned.1.call-start = ((), (), s32[]{:S(2)}) async-start(), calls=%async_computation.2 | async-start | bytes 7864320 | tf_op jit(solution)/shard_map/all_gather | solution.py:23
  16.4 221.2 %copy-start.5 = (f32[768]{0:T(1024)S(1)}, f32[768]{0:T(1024)}, u32[]{:S(2)}) copy-start(f32[768]{0:T(1024)} %param.15) | copy-start | bytes 9220
  16.4 221.1 %copy-start.6 = (f32[768]{0:T(1024)S(1)}, f32[768]{0:T(1024)}, u32[]{:S(2)}) copy-start(f32[768]{0:T(1024)} %param.14) | copy-start | bytes 9220
Sparse Core Ops, SparseCore 0:
  10.7 72.7 all-gather.5
  85.1 82.0 all-gather.3
  169.0 68.5 all-gather.7
where the time goes:
time: 256 us
  waiting for transfers between devices  210 us (82%)
  matrix products  23 us (9%)
  between operations  13.8 us (5%)
  other arithmetic  8.92 us (3%)
    all_gather x1, waiting for transfers between devices, on_device(): piece = lax.all_gather(normed, 'tp', axis=0, tiled=True)  83.7 us
    all_gather x1, waiting for transfers between devices, on_device(): lax.all_gather(gate_cast, 'fs', axis=0, tiled=True)  67.1 us
    all_gather x1, waiting for transfers between devices, on_device(): lax.all_gather(up_cast, 'fs', axis=0, tiled=True)  59.5 us
    dot_general x1, matrix products, on_device(): up = jnp.dot(piece, up_full, preferred_element_type=jnp.float32) * up_scale  12.1 us
    dot_general x1, matrix products, on_device(): jnp.dot(piece, gate_full, preferred_element_type=jnp.float32) * gate_scale  10.9 us
  transfers between devices with their start and end apart: 3, of which 3 were waited for; matrix products, arithmetic and copies ran while one was open for 6% of the time, Pallas kernels for 0%

commit v1 on v0

v1 whole, which is shorter than its diff:
```python
import functools

import jax
import jax.numpy as jnp
from jax import lax
from jax.experimental import pallas as pl
from jax.experimental.pallas import tpu as pltpu
from jax.sharding import PartitionSpec as P

epsilon = 1e-06
CORES = 2
MESH = pl.DeviceIdType.MESH


def rms_scaled(values, gain):
    return values * lax.rsqrt(jnp.mean(values * values, axis=-1, keepdims=True) + epsilon) * gain


def snake(n, i):
    if n % 2:
        return i
    pair = lax.div(i, 2)
    return pair * 2 + lax.rem(lax.rem(i, 2) + pair, 2)


def kernel(
    n, tp, chunk, tile,
    tok_ref, gate_ref, up_ref, gate_scale_ref, up_scale_ref, out_ref,
    tokens, weights, acc, hidden,
    local_sem, ring_send, ring_recv, z_send, z_recv, mate_send, mate_recv, out_sem,
):
    levels = tp // CORES
    rows, width = tok_ref.shape
    depth, cols = gate_ref.shape
    pieces = cols // chunk
    tiles = tp * rows // tile

    fs_i, tp_i = lax.axis_index("fs"), lax.axis_index("tp")
    z, core = lax.div(tp_i, CORES), lax.rem(tp_i, CORES)
    mate = z * CORES + (CORES - 1 - core)
    place = snake(n, fs_i)
    right = snake(n, lax.rem(place + 1, n))
    left = snake(n, lax.rem(place + n - 1, n))
    ring_to = ((right, tp_i), (left, tp_i))

    barrier = pltpu.get_barrier_semaphore()

    def greet(fs_to, tp_to):
        pl.semaphore_signal(barrier, inc=1, device_id=(fs_to, tp_to), device_id_type=MESH)

    greet(right, tp_i)
    greet(left, tp_i)
    greet(fs_i, mate)
    pl.when(z > 0)(lambda: greet(fs_i, tp_i - CORES))
    pl.when(z < levels - 1)(lambda: greet(fs_i, tp_i + CORES))
    pl.semaphore_wait(barrier, 3 + jnp.where(z > 0, 1, 0) + jnp.where(z < levels - 1, 1, 0))

    own = (gate_ref, up_ref)

    def piece(c):
        return pl.ds(c * chunk, chunk)

    def ring(way, hop, c):
        src = own[way].at[:, piece(c)] if hop == 1 else weights.at[way, hop - 1, :, piece(c)]
        return pltpu.make_async_remote_copy(
            src_ref=src,
            dst_ref=weights.at[way, hop, :, piece(c)],
            send_sem=ring_send.at[way, hop - 1, c],
            recv_sem=ring_recv.at[way, hop - 1, c],
            device_id=ring_to[way],
            device_id_type=MESH,
        )

    def block(tp_of):
        return tokens.at[pl.ds(pl.multiple_of(tp_of * rows, rows), rows), :]

    def z_copy(way, distance, source):
        step = CORES if way == 0 else -CORES
        return pltpu.make_async_remote_copy(
            src_ref=tok_ref if distance == 1 else block(source),
            dst_ref=block(source),
            send_sem=z_send.at[way, distance - 1],
            recv_sem=z_recv.at[way, distance - 1],
            device_id=(fs_i, tp_i + step),
            device_id_type=MESH,
        )

    def mate_copy(index, source):
        return pltpu.make_async_remote_copy(
            src_ref=tok_ref if index == 0 else block(source),
            dst_ref=block(source),
            send_sem=mate_send.at[index],
            recv_sem=mate_recv.at[index],
            device_id=(fs_i, mate),
            device_id_type=MESH,
        )

    def mate_index(way, distance):
        return way * (levels - 1) + distance

    def has_source(way, distance):
        return z >= distance if way == 0 else z + distance < levels

    def has_next(way):
        return z < levels - 1 if way == 0 else z > 0

    def source_of(way, distance, tp_of):
        return tp_of - distance * CORES if way == 0 else tp_of + distance * CORES

    for c in range(pieces):
        for way in range(2):
            ring(way, 1, c).start()
    for way in range(2):
        pl.when(has_next(way))(lambda way=way: z_copy(way, 1, tp_i).start())
    mate_copy(0, tp_i).start()
    local = [
        pltpu.make_async_copy(tok_ref, block(tp_i), local_sem.at[0]),
        pltpu.make_async_copy(gate_ref, weights.at[0, 0], local_sem.at[1]),
        pltpu.make_async_copy(up_ref, weights.at[1, 0], local_sem.at[2]),
    ]
    for copy in local:
        copy.start()

    def ring_event(hop, c):
        for way in range(2):
            ring(way, hop, c).wait_recv()
            ring(way, hop + 1, c).start()

    def z_event(distance):
        for way in range(2):
            source = source_of(way, distance, tp_i)

            @pl.when(has_source(way, distance))
            def _():
                z_copy(way, distance, source).wait_recv()
                mate_copy(mate_index(way, distance), source).start()
                if distance < levels - 1:
                    pl.when(has_next(way))(lambda: z_copy(way, distance + 1, source).start())

    ratio = rows * width / (depth * chunk)
    events = [((hop - 1) * pieces + c + 1, functools.partial(ring_event, hop, c))
              for hop in range(1, n - 1) for c in range(pieces)]
    events += [(d * ratio + 0.5, functools.partial(z_event, d)) for d in range(1, levels)]
    for _, event in sorted(events, key=lambda e: e[0]):
        event()

    mate_copy(0, mate).wait_recv()
    for way in range(2):
        for d in range(1, levels):
            pl.when(has_source(way, d))(
                lambda way=way, d=d: mate_copy(mate_index(way, d), source_of(way, d, mate)).wait_recv()
            )
    for copy in local:
        copy.wait()

    def product(way, slot, c, m):
        back = slot if way == 0 else n - slot
        origin = snake(n, lax.rem(place + n - back, n))
        left_side = tokens[
            pl.ds(pl.multiple_of(m * tile, tile), tile),
            pl.ds(pl.multiple_of(origin * depth, depth), depth),
        ]
        right_side = weights[way, slot, :, pl.ds(pl.multiple_of(c * chunk, chunk), chunk)]
        return jnp.dot(left_side, right_side, preferred_element_type=jnp.float32)

    for way in range(2):
        def early(i, carry, way=way):
            c, m = lax.div(i, tiles), lax.rem(i, tiles)
            total = product(way, 0, c, m)
            for slot in range(1, n - 1):
                total += product(way, slot, c, m)
            acc[way, pl.ds(pl.multiple_of(m * tile, tile), tile), pl.ds(pl.multiple_of(c * chunk, chunk), chunk)] = total
            return carry

        lax.fori_loop(0, tiles * pieces, early, 0)

    def out_copy(c):
        return pltpu.make_async_copy(hidden.at[:, piece(c)], out_ref.at[:, piece(c)], out_sem.at[c])

    for c in range(pieces):
        for way in range(2):
            ring(way, n - 1, c).wait_recv()

        def late(m, carry, c=c):
            at = pl.ds(pl.multiple_of(m * tile, tile), tile)
            gate = (acc[0, at, piece(c)] + product(0, n - 1, c, m)) * gate_scale_ref[:, piece(c)]
            up = (acc[1, at, piece(c)] + product(1, n - 1, c, m)) * up_scale_ref[:, piece(c)]
            hidden[at, piece(c)] = (gate / (1.0 + jnp.exp(-gate)) * up).astype(hidden.dtype)
            return carry

        lax.fori_loop(0, tiles, late, 0)
        out_copy(c).start()

    for c in range(pieces):
        for hop in range(1, n):
            for way in range(2):
                ring(way, hop, c).wait_send()
    mate_copy(0, tp_i).wait_send()
    for way in range(2):
        for d in range(1, levels):
            @pl.when(has_source(way, d))
            def _():
                mate_copy(mate_index(way, d), source_of(way, d, tp_i)).wait_send()
        pl.when(has_next(way))(lambda way=way: z_copy(way, 1, tp_i).wait_send())
        for d in range(1, levels - 1):
            @pl.when(has_source(way, d))
            def _():
                pl.when(has_next(way))(
                    lambda: z_copy(way, d + 1, source_of(way, d, tp_i)).wait_send()
                )
    for c in range(pieces):
        out_copy(c).wait()


def solution(mesh):
    n, tp = mesh.shape["fs"], mesh.shape["tp"]

    def on_device(
        stream_in, mixer_out, mix_gain, pre_gain, gate_weight, up_weight, gate_scale, up_scale
    ):
        mixed = stream_in.astype(jnp.float32) + rms_scaled(mixer_out.astype(jnp.float32), mix_gain)
        stream = mixed.astype(jnp.bfloat16)
        normed = rms_scaled(stream.astype(jnp.float32), pre_gain).astype(jnp.bfloat16)
        gate_cast = gate_weight.astype(jnp.bfloat16)
        up_cast = up_weight.astype(jnp.bfloat16)
        rows, width = normed.shape
        depth, cols = gate_cast.shape
        chunk = 256 if cols % 256 == 0 else 128
        tall = tp * rows
        tile = 512 if tall % 512 == 0 else rows
        levels, pieces = tp // CORES, cols // chunk
        anywhere = pl.BlockSpec(memory_space=pl.ANY)
        vmem = pl.BlockSpec(memory_space=pltpu.VMEM)
        dma = pltpu.SemaphoreType.DMA
        hidden = pl.pallas_call(
            functools.partial(kernel, n, tp, chunk, tile),
            out_shape=jax.ShapeDtypeStruct((tall, cols), jnp.bfloat16),
            in_specs=[anywhere] * 3 + [vmem] * 2,
            out_specs=anywhere,
            scratch_shapes=[
                pltpu.VMEM((tall, width), jnp.bfloat16),
                pltpu.VMEM((2, n, depth, cols), jnp.bfloat16),
                pltpu.VMEM((2, tall, cols), jnp.float32),
                pltpu.VMEM((tall, cols), jnp.bfloat16),
                dma((3,)),
                dma((2, n - 1, pieces)),
                dma((2, n - 1, pieces)),
                dma((2, levels)),
                dma((2, levels)),
                dma((2 * levels,)),
                dma((2 * levels,)),
                dma((pieces,)),
            ],
            compiler_params=pltpu.CompilerParams(
                collective_id=0, has_side_effects=True, vmem_limit_bytes=60 * 1024 * 1024
            ),
        )(normed, gate_cast, up_cast, gate_scale.reshape(1, -1), up_scale.reshape(1, -1))
        return (hidden, stream)

    return jax.shard_map(
        on_device,
        mesh=mesh,
        in_specs=(
            P(("fs", "tp"), None),
            P(("fs", "tp"), None),
            P(),
            P(),
            P("fs", "tp"),
            P("fs", "tp"),
            P("tp"),
            P("tp"),
        ),
        out_specs=(P("fs", "tp"), P(("fs", "tp"), None)),
        check_vma=False,
    )
```

time: 256 us -> 125 us (0.49)
  waiting for transfers between devices: 210 us -> 0 us
  Pallas kernels: 0 us -> 110 us
  matrix products: 23 us -> 0 us
  between operations: 13.8 us -> 0.68 us
  local copies, waits for them, and re-layouts: 0.04 us -> 6.39 us
    all_gather x3 -> x0, waiting for transfers between devices: 210 us -> none  [the longest x1 83.7 us: on_device(): piece = lax.all_gather(normed, 'tp', axis=0, tiled=True)]
    pallas_call x0 -> x1, Pallas kernels: none -> 110 us  [on_device(): pl.pallas_call(functools.partial(kernel, n, tp, chunk, tile), out_shape=j...]
    dot_general x2 -> x0, matrix products: 23 us -> none  [the longest x1 12.1 us: on_device(): up = jnp.dot(piece, up_full, preferred_element_type=jnp.float32) * up_scale]
    unnamed x14 -> x9, local copies, waits for them, and re-layouts: 0.04 us -> 3.82 us
    reduce_sum x2, other arithmetic: 1.03 us -> 3.97 us  [rms_scaled(): jnp.mean(values * values, axis=-1, keepdims=True) + epsilon]
    reshape x0 -> x2, local copies, waits for them, and re-layouts: none -> 2.57 us  [the longest x1 1.29 us: on_device(): gate_scale.reshape(1, -1)]
  transfers between devices with their start and end apart: 3 -> 0, of which waited for: 3 -> 0; matrix products, arithmetic and copies ran while one was open for 6% -> 0% of each run, Pallas kernels for 0% -> 0%
where the time goes in v1:
time: 125 us
  Pallas kernels  110 us (88%)
  other arithmetic  7.89 us (6%)
  local copies, waits for them, and re-layouts  6.39 us (5%)
    pallas_call x1, Pallas kernels, on_device(): pl.pallas_call(functools.partial(kernel, n, tp, chunk, tile), out_shape=j...  110 us
    reduce_sum x2, other arithmetic, rms_scaled(): jnp.mean(values * values, axis=-1, keepdims=True) + epsilon  3.97 us
    unnamed x9, local copies, waits for them, and re-layouts  3.82 us

profile of v1, /device:TPU:0, one launch (start us, length us, event | category | flops | bytes accessed | tf_op | source)
XLA Modules:
  0.0 125.0 jit_solution(7280923733908742508)
XLA Ops:
  0.6 0.0 copy-start.3
  0.6 1.5 %fusion = f32[128]{0:T(128)S(1)} fusion(bf16[128,4096]{1,0:T(8,128)(2,1)} %param.9), kind=kLoop, calls=%fused_computation.4 | loop fusion | flops 1572736 | bytes 1049088 | tf_op jit(solution)/shard_map/reduce_sum | solution.py:16
  2.2 1.3 %reshape.28.gate_scale_ref = f32[1,768]{1,0:T(1,128)} reshape(f32[768]{0:T(1024)} %param.14) | data formatting | bytes 6144 | tf_op jit(solution)/shard_map/reshape | solution.py:257
  3.5 1.3 %reshape.29.up_scale_ref = f32[1,768]{1,0:T(1,128)} reshape(f32[768]{0:T(1024)} %param.15) | data formatting | bytes 6144 | tf_op jit(solution)/shard_map/reshape | solution.py:257
  4.7 0.0 copy-start.1
  4.7 2.4 %fusion.4 = (f32[128]{0:T(128)S(1)}, bf16[128,4096]{1,0:T(8,128)(2,1)S(1)}) fusion(f32[4096]{0:T(1024)} %param.10, f32[128]{0:T(128)S(1)} %add_rsqrt_fusion.1, bf16[128,4096]{1,0:T(8,128)(2,1)} %param.9, bf16[128,4096]{1,0:T(8,128)(2,1)} %param.8), kind=kLoop, calls=%fused_computation.8 | loop fusion | flops 4718464 | bytes 3163136 | tf_op jit(solution)/shard_map/reduce_sum | solution.py:16
  7.2 0.0 copy-start
  7.2 0.0 copy-done.3
  7.2 1.3 %fusion.6.tok_ref = bf16[128,4096]{1,0:T(8,128)(2,1)} fusion(bf16[128,4096]{1,0:T(8,128)(2,1)S(1)} %get-tuple-element.7, f32[4096]{0:T(1024)S(1)} %copy-done.3, f32[128]{0:T(128)S(1)} %add_rsqrt_fusion), kind=kLoop, calls=%fused_computation.10 | loop fusion | flops 2097152 | bytes 2114048 | tf_op jit(solution)/shard_map/convert_element_type | solution.py:223
  8.5 0.0 copy-done.1
  8.5 0.0 copy-start.2
  8.5 1.3 %convert_element_type.26.gate_ref = bf16[1024,768]{1,0:T(8,128)(2,1)} convert(f32[1024,768]{1,0:T(8,128)S(1)} %copy-done.1) | non-fusion elementwise | flops 786432 | bytes 4718592 | tf_op jit(solution)/shard_map/convert_element_type | solution.py:224
  9.8 0.0 copy-done
  9.8 1.2 copy-done.2
  11.0 1.3 %convert_element_type.27.up_ref = bf16[1024,768]{1,0:T(8,128)(2,1)} convert(f32[1024,768]{1,0:T(8,128)S(1)} %copy-done.2) | non-fusion elementwise | flops 786432 | bytes 4718592 | tf_op jit(solution)/shard_map/convert_element_type | solution.py:225
  12.3 110.1 %shard_map.95 = bf16[1024,768]{1,0:T(8,128)(2,1)} custom-call(bf16[128,4096]{1,0:T(8,128)(2,1)} %fusion.6.tok_ref, bf16[1024,768]{1,0:T(8,128)(2,1)} %convert_element_type.26.gate_ref, bf16[1024,768]{1,0:T(8,128)(2,1)} %convert_element_type.27.up_ref, f32[1,768]{1,0:T(1,128)} %reshape.28.gate_scale_ref, f32[1,768]{1,0:T(1,128)} %reshape.29.up_scale_ref), custom_call_target="tpu_custom_call" | custom-call | tf_op jit(solution)/shard_map/pallas_call | solution.py:235
  122.4 2.7 %copy.11 = bf16[1024,768]{1,0:T(8,128)(2,1)} copy(bf16[1024,768]{1,0:T(8,128)(2,1)} %shard_map.95) | data formatting | bytes 3145728
  (2 shorter events, 0.0 us)
Async XLA Ops:
  0.6 6.6 %copy-start.3 = (f32[4096]{0:T(1024)S(1)}, f32[4096]{0:T(1024)}, u32[]{:S(2)}) copy-start(f32[4096]{0:T(1024)} %param.11) | copy-start | bytes 49156
  4.7 3.8 %copy-start.1 = (f32[1024,768]{1,0:T(8,128)S(1)}, f32[1024,768]{1,0:T(8,128)}, u32[]{:S(2)}) copy-start(f32[1024,768]{1,0:T(8,128)} %param.12) | copy-start | bytes 9437188
  7.2 2.6 %copy-start = (bf16[128,4096]{1,0:T(8,128)(2,1)}, bf16[128,4096]{1,0:T(8,128)(2,1)S(1)}, u32[]{:S(2)}) copy-start(bf16[128,4096]{1,0:T(8,128)(2,1)S(1)} %get-tuple-element.7) | copy-start | bytes 3145732
  8.5 2.5 %copy-start.2 = (f32[1024,768]{1,0:T(8,128)S(1)}, f32[1024,768]{1,0:T(8,128)}, u32[]{:S(2)}) copy-start(f32[1024,768]{1,0:T(8,128)} %param.13) | copy-start | bytes 9437188

commit v2 on v1

--- a/solution.py
+++ b/solution.py
@@ -9,6 +9,7 @@
 
 epsilon = 1e-06
 CORES = 2
+ROWS = 16
 MESH = pl.DeviceIdType.MESH
 
 
@@ -25,14 +26,16 @@
 
 def kernel(
     n, tp, chunk, tile,
-    tok_ref, gate_ref, up_ref, gate_scale_ref, up_scale_ref, out_ref,
-    tokens, weights, acc, hidden,
-    local_sem, ring_send, ring_recv, z_send, z_recv, mate_send, mate_recv, out_sem,
+    stream_ref, mixer_ref, mix_gain_ref, pre_gain_ref, gate_ref, up_ref, gate_scale_ref, up_scale_ref,
+    hidden, stream_out,
+    tokens, weights, acc, wide, stream_in, mixer,
+    row_sem, wide_sem, ring_send, ring_recv, z_send, z_recv, mate_send, mate_recv,
 ):
     levels = tp // CORES
-    rows, width = tok_ref.shape
+    rows, width = stream_ref.shape
     depth, cols = gate_ref.shape
     pieces = cols // chunk
+    strip = min(depth, 128)
     tiles = tp * rows // tile
 
     fs_i, tp_i = lax.axis_index("fs"), lax.axis_index("tp")
@@ -43,6 +46,28 @@
     left = snake(n, lax.rem(place + n - 1, n))
     ring_to = ((right, tp_i), (left, tp_i))
 
+    def piece(c):
+        return pl.ds(c * chunk, chunk)
+
+    source = (gate_ref, up_ref)
+
+    def wide_copy(way, c):
+        return pltpu.make_async_copy(
+            source[way].at[:, piece(c)], wide.at[way, :, piece(c)], wide_sem.at[way, c]
+        )
+
+    row_copies = (
+        pltpu.make_async_copy(stream_ref, stream_in, row_sem.at[0]),
+        pltpu.make_async_copy(mixer_ref, mixer, row_sem.at[1]),
+    )
+    for way in range(2):
+        wide_copy(way, 0).start()
+    for copy in row_copies:
+        copy.start()
+    for c in range(1, pieces):
+        for way in range(2):
+            wide_copy(way, c).start()
+
     barrier = pltpu.get_barrier_semaphore()
 
     def greet(fs_to, tp_to):
@@ -53,17 +78,24 @@
     greet(fs_i, mate)
     pl.when(z > 0)(lambda: greet(fs_i, tp_i - CORES))
     pl.when(z < levels - 1)(lambda: greet(fs_i, tp_i + CORES))
+
+    def cast(c):
+        for way in range(2):
+            wide_copy(way, c).wait()
+
+            def some(i, carry, way=way):
+                at = pl.ds(pl.multiple_of(i * strip, strip), strip)
+                weights[way, 0, at, piece(c)] = wide[way, at, piece(c)].astype(weights.dtype)
+                return carry
+
+            lax.fori_loop(0, depth // strip, some, 0)
+
+    cast(0)
     pl.semaphore_wait(barrier, 3 + jnp.where(z > 0, 1, 0) + jnp.where(z < levels - 1, 1, 0))
 
-    own = (gate_ref, up_ref)
-
-    def piece(c):
-        return pl.ds(c * chunk, chunk)
-
     def ring(way, hop, c):
-        src = own[way].at[:, piece(c)] if hop == 1 else weights.at[way, hop - 1, :, piece(c)]
         return pltpu.make_async_remote_copy(
-            src_ref=src,
+            src_ref=weights.at[way, hop - 1, :, piece(c)],
             dst_ref=weights.at[way, hop, :, piece(c)],
             send_sem=ring_send.at[way, hop - 1, c],
             recv_sem=ring_recv.at[way, hop - 1, c],
@@ -77,7 +109,7 @@
     def z_copy(way, distance, source):
         step = CORES if way == 0 else -CORES
         return pltpu.make_async_remote_copy(
-            src_ref=tok_ref if distance == 1 else block(source),
+            src_ref=block(source),
             dst_ref=block(source),
             send_sem=z_send.at[way, distance - 1],
             recv_sem=z_recv.at[way, distance - 1],
@@ -87,7 +119,7 @@
 
     def mate_copy(index, source):
         return pltpu.make_async_remote_copy(
-            src_ref=tok_ref if index == 0 else block(source),
+            src_ref=block(source),
             dst_ref=block(source),
             send_sem=mate_send.at[index],
             recv_sem=mate_recv.at[index],
@@ -107,19 +139,33 @@
     def source_of(way, distance, tp_of):
         return tp_of - distance * CORES if way == 0 else tp_of + distance * CORES
 
-    for c in range(pieces):
-        for way in range(2):
-            ring(way, 1, c).start()
+    for way in range(2):
+        ring(way, 1, 0).start()
+
+    for copy in row_copies:
+        copy.wait()
+    mix_gain, pre_gain = mix_gain_ref[...].reshape(1, -1), pre_gain_ref[...].reshape(1, -1)
+
+    def norm(i, carry):
+        at = pl.ds(pl.multiple_of(i * ROWS, ROWS), ROWS)
+        mixed = stream_in[at, :].astype(jnp.float32) + rms_scaled(
+            mixer[at, :].astype(jnp.float32), mix_gain
+        )
+        stream = mixed.astype(stream_out.dtype)
+        stream_out[at, :] = stream
+        own_at = pl.ds(pl.multiple_of(tp_i * rows + i * ROWS, ROWS), ROWS)
+        tokens[own_at, :] = rms_scaled(stream.astype(jnp.float32), pre_gain).astype(tokens.dtype)
+        return carry
+
+    lax.fori_loop(0, rows // ROWS, norm, 0)
+    for c in range(1, pieces):
+        cast(c)
     for way in range(2):
         pl.when(has_next(way))(lambda way=way: z_copy(way, 1, tp_i).start())
     mate_copy(0, tp_i).start()
-    local = [
-        pltpu.make_async_copy(tok_ref, block(tp_i), local_sem.at[0]),
-        pltpu.make_async_copy(gate_ref, weights.at[0, 0], local_sem.at[1]),
-        pltpu.make_async_copy(up_ref, weights.at[1, 0], local_sem.at[2]),
-    ]
-    for copy in local:
-        copy.start()
+    for c in range(1, pieces):
+        for way in range(2):
+            ring(way, 1, c).start()
 
     def ring_event(hop, c):
         for way in range(2):
@@ -150,8 +196,6 @@
             pl.when(has_source(way, d))(
                 lambda way=way, d=d: mate_copy(mate_index(way, d), source_of(way, d, mate)).wait_recv()
             )
-    for copy in local:
-        copy.wait()
 
     def product(way, slot, c, m):
         back = slot if way == 0 else n - slot
@@ -174,22 +218,19 @@
 
         lax.fori_loop(0, tiles * pieces, early, 0)
 
-    def out_copy(c):
-        return pltpu.make_async_copy(hidden.at[:, piece(c)], out_ref.at[:, piece(c)], out_sem.at[c])
-
+    gate_scale, up_scale = gate_scale_ref[...].reshape(1, -1), up_scale_ref[...].reshape(1, -1)
     for c in range(pieces):
         for way in range(2):
             ring(way, n - 1, c).wait_recv()
 
         def late(m, carry, c=c):
             at = pl.ds(pl.multiple_of(m * tile, tile), tile)
-            gate = (acc[0, at, piece(c)] + product(0, n - 1, c, m)) * gate_scale_ref[:, piece(c)]
-            up = (acc[1, at, piece(c)] + product(1, n - 1, c, m)) * up_scale_ref[:, piece(c)]
+            gate = (acc[0, at, piece(c)] + product(0, n - 1, c, m)) * gate_scale[:, c * chunk:(c + 1) * chunk]
+            up = (acc[1, at, piece(c)] + product(1, n - 1, c, m)) * up_scale[:, c * chunk:(c + 1) * chunk]
             hidden[at, piece(c)] = (gate / (1.0 + jnp.exp(-gate)) * up).astype(hidden.dtype)
             return carry
 
         lax.fori_loop(0, tiles, late, 0)
-        out_copy(c).start()
 
     for c in range(pieces):
         for hop in range(1, n):
@@ -208,8 +249,6 @@
                 pl.when(has_next(way))(
                     lambda: z_copy(way, d + 1, source_of(way, d, tp_i)).wait_send()
                 )
-    for c in range(pieces):
-        out_copy(c).wait()
 
 
 def solution(mesh):
@@ -218,13 +257,7 @@
     def on_device(
         stream_in, mixer_out, mix_gain, pre_gain, gate_weight, up_weight, gate_scale, up_scale
     ):
-        mixed = stream_in.astype(jnp.float32) + rms_scaled(mixer_out.astype(jnp.float32), mix_gain)
-        stream = mixed.astype(jnp.bfloat16)
-        normed = rms_scaled(stream.astype(jnp.float32), pre_gain).astype(jnp.bfloat16)
-        gate_cast = gate_weight.astype(jnp.bfloat16)
-        up_cast = up_weight.astype(jnp.bfloat16)
-        rows, width = normed.shape
-        depth, cols = gate_cast.shape
+        (rows, width), (depth, cols) = stream_in.shape, gate_weight.shape
         chunk = 256 if cols % 256 == 0 else 128
         tall = tp * rows
         tile = 512 if tall % 512 == 0 else rows
@@ -232,30 +265,37 @@
         anywhere = pl.BlockSpec(memory_space=pl.ANY)
         vmem = pl.BlockSpec(memory_space=pltpu.VMEM)
         dma = pltpu.SemaphoreType.DMA
-        hidden = pl.pallas_call(
+        return pl.pallas_call(
             functools.partial(kernel, n, tp, chunk, tile),
-            out_shape=jax.ShapeDtypeStruct((tall, cols), jnp.bfloat16),
-            in_specs=[anywhere] * 3 + [vmem] * 2,
-            out_specs=anywhere,
+            out_shape=(
+                jax.ShapeDtypeStruct((tall, cols), jnp.bfloat16),
+                jax.ShapeDtypeStruct((rows, width), jnp.bfloat16),
+            ),
+            in_specs=[anywhere] * 2 + [vmem] * 2 + [anywhere] * 2 + [vmem] * 2,
+            out_specs=(vmem, vmem),
             scratch_shapes=[
                 pltpu.VMEM((tall, width), jnp.bfloat16),
                 pltpu.VMEM((2, n, depth, cols), jnp.bfloat16),
                 pltpu.VMEM((2, tall, cols), jnp.float32),
-                pltpu.VMEM((tall, cols), jnp.bfloat16),
-                dma((3,)),
+                pltpu.VMEM((2, depth, cols), jnp.float32),
+                pltpu.VMEM((rows, width), jnp.bfloat16),
+                pltpu.VMEM((rows, width), jnp.bfloat16),
+                dma((2,)),
+                dma((2, pieces)),
                 dma((2, n - 1, pieces)),
                 dma((2, n - 1, pieces)),
                 dma((2, levels)),
                 dma((2, levels)),
                 dma((2 * levels,)),
                 dma((2 * levels,)),
-                dma((pieces,)),
             ],
             compiler_params=pltpu.CompilerParams(
-                collective_id=0, has_side_effects=True, vmem_limit_bytes=60 * 1024 * 1024
+                collective_id=0, has_side_effects=True, vmem_limit_bytes=48 * 1024 * 1024
             ),
-        )(normed, gate_cast, up_cast, gate_scale.reshape(1, -1), up_scale.reshape(1, -1))
-        return (hidden, stream)
+        )(
+            stream_in, mixer_out, mix_gain, pre_gain,
+            gate_weight, up_weight, gate_scale, up_scale,
+        )
 
     return jax.shard_map(
         on_device,

time: 125 us -> 117 us (0.936)
  other arithmetic: 7.89 us -> 0 us
    reduce_sum x2 -> x0, other arithmetic: 3.97 us -> none  [rms_scaled(): jnp.mean(values * values, axis=-1, keepdims=True) + epsilon]
    convert_element_type x3 -> x0, other arithmetic: 3.91 us -> none  [the longest x1 1.31 us: on_device(): rms_scaled(stream.astype(jnp.float32), pre_gain).astype(jnp.bfloat16)]
    unnamed x9 -> x14, local copies, waits for them, and re-layouts: 3.82 us -> 7.36 us
    reshape x2 -> x0, local copies, waits for them, and re-layouts: 2.57 us -> none  [the longest x1 1.29 us: on_device(): gate_scale.reshape(1, -1)]
    pallas_call x1, Pallas kernels: 110 us -> 109 us  [on_device(): pl.pallas_call(functools.partial(kernel, n, tp, chunk, tile), out_shape=(...]
where the time goes in v2:
time: 117 us
  Pallas kernels  109 us (93%)
  local copies, waits for them, and re-layouts  7.36 us (6%)
    pallas_call x1, Pallas kernels, on_device(): pl.pallas_call(functools.partial(kernel, n, tp, chunk, tile), out_shape=(...  109 us
    unnamed x14, local copies, waits for them, and re-layouts  7.36 us

profile of v2, /device:TPU:0, one launch (start us, length us, event | category | flops | bytes accessed | tf_op | source)
XLA Modules:
  0.0 116.7 jit_solution(230421185539086801)
XLA Ops:
  0.6 0.0 copy-start
  0.6 1.2 %copy-done = bf16[128,4096]{1,0:T(8,128)(2,1)S(1)} copy-done((bf16[128,4096]{1,0:T(8,128)(2,1)S(1)}, bf16[128,4096]{1,0:T(8,128)(2,1)}, u32[]{:S(2)}) %copy-start) | copy-done | bytes 1048600
  1.9 0.0 copy-start.1
  1.9 1.2 %copy-done.1 = bf16[128,4096]{1,0:T(8,128)(2,1)S(1)} copy-done((bf16[128,4096]{1,0:T(8,128)(2,1)S(1)}, bf16[128,4096]{1,0:T(8,128)(2,1)}, u32[]{:S(2)}) %copy-start.1) | copy-done | bytes 1048600
  3.1 0.0 copy-start.2
  3.1 0.7 copy-done.2
  3.8 0.0 copy-start.3
  3.8 0.7 copy-done.3
  4.5 0.0 copy-start.4
  4.5 0.7 copy-done.4
  5.2 0.0 copy-start.5
  5.2 0.7 copy-done.5
  5.9 108.7 %shard_map.95 = (bf16[1024,768]{1,0:T(8,128)(2,1)S(1)}, bf16[128,4096]{1,0:T(8,128)(2,1)S(1)}) custom-call(bf16[128,4096]{1,0:T(8,128)(2,1)S(1)} %copy-done, bf16[128,4096]{1,0:T(8,128)(2,1)S(1)} %copy-done.1, f32[4096]{0:T(1024)S(1)} %copy-done.2, f32[4096]{0:T(1024)S(1)} %copy-done.3, f32[1024,768]{1,0:T(8,128)} %gate_ref.1, f32[1024,768]{1,0:T(8,128)} %up_ref.1, ...), custom_call_target="tpu_custom_call" | custom-call | tf_op jit(solution)/shard_map/pallas_call | solution.py:268
  114.6 1.1 copy.12
  115.8 1.0 copy.13
Async XLA Ops:
  0.6 1.2 %copy-start = (bf16[128,4096]{1,0:T(8,128)(2,1)S(1)}, bf16[128,4096]{1,0:T(8,128)(2,1)}, u32[]{:S(2)}) copy-start(bf16[128,4096]{1,0:T(8,128)(2,1)} %stream_ref.1) | copy-start | bytes 3145732
  1.9 1.2 %copy-start.1 = (bf16[128,4096]{1,0:T(8,128)(2,1)S(1)}, bf16[128,4096]{1,0:T(8,128)(2,1)}, u32[]{:S(2)}) copy-start(bf16[128,4096]{1,0:T(8,128)(2,1)} %mixer_ref.1) | copy-start | bytes 3145732
  3.1 0.7 copy-start.2
  3.8 0.7 copy-start.3
  4.5 0.7 copy-start.4
  5.2 0.7 copy-start.5

commit v3 on v2

--- a/solution.py
+++ b/solution.py
@@ -28,7 +28,7 @@
     n, tp, chunk, tile,
     stream_ref, mixer_ref, mix_gain_ref, pre_gain_ref, gate_ref, up_ref, gate_scale_ref, up_scale_ref,
     hidden, stream_out,
-    tokens, weights, acc, wide, stream_in, mixer,
+    tokens, weights, acc, wide, stream_in, mixer, gains, scales,
     row_sem, wide_sem, ring_send, ring_recv, z_send, z_recv, mate_send, mate_recv,
 ):
     levels = tp // CORES
@@ -59,6 +59,10 @@
     row_copies = (
         pltpu.make_async_copy(stream_ref, stream_in, row_sem.at[0]),
         pltpu.make_async_copy(mixer_ref, mixer, row_sem.at[1]),
+        pltpu.make_async_copy(mix_gain_ref, gains[0], row_sem.at[2]),
+        pltpu.make_async_copy(pre_gain_ref, gains[1], row_sem.at[3]),
+        pltpu.make_async_copy(gate_scale_ref, scales[0], row_sem.at[4]),
+        pltpu.make_async_copy(up_scale_ref, scales[1], row_sem.at[5]),
     )
     for way in range(2):
         wide_copy(way, 0).start()
@@ -144,7 +148,7 @@
 
     for copy in row_copies:
         copy.wait()
-    mix_gain, pre_gain = mix_gain_ref[...].reshape(1, -1), pre_gain_ref[...].reshape(1, -1)
+    mix_gain, pre_gain = (gain[...].reshape(1, -1) for gain in gains)
 
     def norm(i, carry):
         at = pl.ds(pl.multiple_of(i * ROWS, ROWS), ROWS)
@@ -218,7 +222,7 @@
 
         lax.fori_loop(0, tiles * pieces, early, 0)
 
-    gate_scale, up_scale = gate_scale_ref[...].reshape(1, -1), up_scale_ref[...].reshape(1, -1)
+    gate_scale, up_scale = (scale[...].reshape(1, -1) for scale in scales)
     for c in range(pieces):
         for way in range(2):
             ring(way, n - 1, c).wait_recv()
@@ -262,7 +266,7 @@
         tall = tp * rows
         tile = 512 if tall % 512 == 0 else rows
         levels, pieces = tp // CORES, cols // chunk
-        anywhere = pl.BlockSpec(memory_space=pl.ANY)
+        hbm = pl.BlockSpec(memory_space=pltpu.HBM)
         vmem = pl.BlockSpec(memory_space=pltpu.VMEM)
         dma = pltpu.SemaphoreType.DMA
         return pl.pallas_call(
@@ -271,7 +275,7 @@
                 jax.ShapeDtypeStruct((tall, cols), jnp.bfloat16),
                 jax.ShapeDtypeStruct((rows, width), jnp.bfloat16),
             ),
-            in_specs=[anywhere] * 2 + [vmem] * 2 + [anywhere] * 2 + [vmem] * 2,
+            in_specs=[hbm] * 8,
             out_specs=(vmem, vmem),
             scratch_shapes=[
                 pltpu.VMEM((tall, width), jnp.bfloat16),
@@ -280,7 +284,9 @@
                 pltpu.VMEM((2, depth, cols), jnp.float32),
                 pltpu.VMEM((rows, width), jnp.bfloat16),
                 pltpu.VMEM((rows, width), jnp.bfloat16),
-                dma((2,)),
+                (pltpu.VMEM((width,), jnp.float32),) * 2,
+                (pltpu.VMEM((cols,), jnp.float32),) * 2,
+                dma((6,)),
                 dma((2, pieces)),
                 dma((2, n - 1, pieces)),
                 dma((2, n - 1, pieces)),
@@ -290,7 +296,7 @@
                 dma((2 * levels,)),
             ],
             compiler_params=pltpu.CompilerParams(
-                collective_id=0, has_side_effects=True, vmem_limit_bytes=48 * 1024 * 1024
+                collective_id=0, has_side_effects=True, vmem_limit_bytes=57 * 1024 * 1024
             ),
         )(
             stream_in, mixer_out, mix_gain, pre_gain,

time: 117 us -> 115 us (0.983)
  local copies, waits for them, and re-layouts: 7.36 us -> 3.71 us
  Pallas kernels: 109 us -> 111 us
    unnamed x14 -> x4, local copies, waits for them, and re-layouts: 7.36 us -> 3.71 us
    pallas_call x1, Pallas kernels: 109 us -> 111 us  [on_device(): pl.pallas_call(functools.partial(kernel, n, tp, chunk, tile), out_shape=(...]
where the time goes in v3:
time: 115 us
  Pallas kernels  111 us (97%)
  local copies, waits for them, and re-layouts  3.71 us (3%)
    pallas_call x1, Pallas kernels, on_device(): pl.pallas_call(functools.partial(kernel, n, tp, chunk, tile), out_shape=(...  111 us
    unnamed x4, local copies, waits for them, and re-layouts  3.71 us

profile of v3, /device:TPU:0, one launch (start us, length us, event | category | flops | bytes accessed | tf_op | source)
XLA Modules:
  0.0 115.0 jit_solution(16221074703222736270)
XLA Ops:
  0.6 110.6 %shard_map.95 = (bf16[1024,768]{1,0:T(8,128)(2,1)}, bf16[128,4096]{1,0:T(8,128)(2,1)}) custom-call(bf16[128,4096]{1,0:T(8,128)(2,1)} %stream_ref.1, bf16[128,4096]{1,0:T(8,128)(2,1)} %mixer_ref.1, f32[4096]{0:T(1024)} %mix_gain_ref.1, f32[4096]{0:T(1024)} %pre_gain_ref.1, f32[1024,768]{1,0:T(8,128)} %gate_ref.1, f32[1024,768]{1,0:T(8,128)} %up_ref.1, ...), custom_call_target="tpu_custom_call" | custom-call | tf_op jit(solution)/shard_map/pallas_call | solution.py:272
  111.3 0.0 copy-start
  111.3 2.7 %copy.12 = bf16[1024,768]{1,0:T(8,128)(2,1)} copy(bf16[1024,768]{1,0:T(8,128)(2,1)} %get-tuple-element.4) | data formatting | bytes 3145728
  114.0 0.0 copy-done
  114.0 1.0 copy.13
Async XLA Ops:
  111.3 2.8 %copy-start = (bf16[128,4096]{1,0:T(8,128)(2,1)S(1)}, bf16[128,4096]{1,0:T(8,128)(2,1)}, u32[]{:S(2)}) copy-start(bf16[128,4096]{1,0:T(8,128)(2,1)} %get-tuple-element.5) | copy-start | bytes 3145732
